TPU v7x, 32 devices: a whole 2x2x4 slice. The times are simulated.
32 devices in a mesh: grp: 2 (over y), sp: 4 (over z), tp: 4 (over x, core).
Axes of the slice: x: 2, y: 2, z: 4, core: 2. Of those that a mesh axis runs over, the one named last changes fastest.
Arguments:
- tokens: bfloat16 [4096, 4096], P(('grp', 'sp', 'tp')), parts along dimension 0, may hold values from -6 to 6
- norm_gain: float32 [4096], replicated, may hold values from 0.1 to 1.9
- query_diff: bfloat16 [4096, 2048], P('sp', 'tp'), may hold values from -1.25 to 1.25
- key_diff: bfloat16 [4096, 2048], P('sp', 'tp'), may hold values from -1.25 to 1.25
- value_diff: bfloat16 [4096, 2048], P('sp', 'tp'), may hold values from -0.09375 to 0.09375
- lam: float32 [8], P('tp'), may hold values from 0.3 to 0.8
- output_norm_gain: float32 [256], replicated, may hold values from 0.1 to 1.9
- query_win: bfloat16 [4096, 2048], P('sp', 'tp'), may hold values from -1.25 to 1.25
- keyval_win: bfloat16 [4, 4096, 256], P(None, 'sp'), may hold values from -1.25 to 1.25
- sink: float32 [16], P('tp'), may hold values from 4 to 7
- proj_diff: bfloat16 [2048, 4096], P('tp'), may hold values from -0.125 to 0.125
- proj_win: bfloat16 [2048, 4096], P('tp'), may hold values from -0.79296875 to 0.79296875
Outputs:
- mixed: bfloat16 [4096, 4096], P(('grp', 'sp', 'tp')), parts along dimension 0
There are 2 independent parts, one for each index of `grp`. A program takes and returns all parts, laid end to end along the dimension named above; an argument that names none is the same for every part. Nothing has to cross between parts.
All inputs are finite; a program needn't handle non-finite values.
Results may differ from a plain program's by a relative error of at most 0.015.
Values may be sent and summed in bfloat16 or wider, within the bound.
A program may use at most 128 MiB of HBM per device.

v0:
```python
import math

import jax
import jax.numpy as jnp
from jax import lax
from jax.sharding import PartitionSpec as P

HEAD = 128
WIN_HEADS = 16
KV_HEADS = 4
WINDOW = 128
VDIM = 256


EPS = 1e-06


def padded_2(x, sides, width):
    for axis, dim in sides:
        devices, length = (lax.axis_size(axis), x.shape[dim])
        up = [(i, (i + 1) % devices) for i in range(devices - 1)]
        down = [(j, i) for i, j in up]
        last = lax.slice_in_dim(x, length - width, length, axis=dim)
        first = lax.slice_in_dim(x, 0, width, axis=dim)
        before = lax.ppermute(last, axis, up)
        after = lax.ppermute(first, axis, down)
        x = jnp.concatenate([before, x, after], axis=dim)
    return x


def root_mean_square_rows(values, gain):
    return values * lax.rsqrt(jnp.mean(values * values, axis=-1, keepdims=True) + EPS) * gain


def body(
    tokens,
    norm_gain,
    query_diff,
    key_diff,
    value_diff,
    lam,
    output_norm_gain,
    query_win,
    keyval_win,
    sink,
    proj_diff,
    proj_win,
):
    normed = root_mean_square_rows(tokens.astype(jnp.float32), norm_gain).astype(jnp.bfloat16)
    heads_diff = lam.shape[0]
    heads_win = sink.shape[0]
    group = WIN_HEADS // KV_HEADS
    kv_index = lax.axis_index("tp") * heads_win // group
    kv_local = lax.dynamic_index_in_dim(keyval_win, kv_index, 0, keepdims=False)
    pieces = [query_diff, key_diff, value_diff, query_win, kv_local]
    stacked = jnp.concatenate(pieces, axis=1)
    whole = lax.all_gather(stacked, "sp", axis=0, tiled=True)
    projected = jnp.dot(
        lax.all_gather(normed, "tp", axis=0, tiled=True), whole, preferred_element_type=jnp.float32
    )
    projected = projected.astype(jnp.bfloat16)
    output_list = []
    offset = 0
    for piece in pieces:
        output_list.append(projected[:, offset : offset + piece.shape[1]])
        offset = offset + piece.shape[1]
    q_diff, k_diff, v_diff, q_win, kv_win = output_list
    tok = projected.shape[0]
    scale = HEAD ** (-0.5)
    q_four = q_diff.reshape(tok, heads_diff, 2, HEAD)
    start_state = (
        jnp.full((heads_diff, 2, tok), -jnp.inf, jnp.float32),
        jnp.zeros((heads_diff, 2, tok), jnp.float32),
        jnp.zeros((heads_diff, 2, tok, VDIM), jnp.float32),
    )
    carry = start_state
    keys = lax.all_gather(k_diff, "sp", axis=0, tiled=True)
    values = lax.all_gather(v_diff, "sp", axis=0, tiled=True)
    rows = keys.shape[0]
    step = math.gcd(rows, 1024)
    key_blocks = keys.reshape(rows // step, step, heads_diff, 2, HEAD)
    value_blocks = values.reshape(rows // step, step, heads_diff, VDIM)

    def one(state, block):
        top, total, acc = state
        key_part, value_part = block
        scores = (
            jnp.einsum("qhmd,khmd->hmqk", q_four, key_part, preferred_element_type=jnp.float32)
            * scale
        )
        new_top = jnp.maximum(top, jnp.max(scores, axis=-1))
        expo = jnp.exp(scores - new_top[..., None])
        fade = jnp.exp(top - new_top)
        total = total * fade + jnp.sum(expo, axis=-1)
        acc = acc * fade[..., None] + jnp.einsum(
            "hmqk,khe->hmqe",
            expo.astype(jnp.bfloat16),
            value_part,
            preferred_element_type=jnp.float32,
        )
        return ((new_top, total, acc), None)

    carry, unused = lax.scan(one, carry, (key_blocks, value_blocks))
    top, total, acc = carry
    attention_maps = acc / total[..., None]
    difference_output = attention_maps[:, 0] - lam[:, None, None] * attention_maps[:, 1]
    differential_output = root_mean_square_rows(difference_output, output_norm_gain).astype(
        jnp.bfloat16
    )
    differential_output = jnp.transpose(differential_output, (1, 0, 2)).reshape(
        tok, heads_diff * VDIM
    )
    padded = padded_2(kv_win, (("sp", 0),), WINDOW)
    nblocks = tok // WINDOW
    blocks = padded.reshape(nblocks + 2, WINDOW, 2 * HEAD)
    band = jnp.concatenate([blocks[:-2], blocks[1:-1], blocks[2:]], axis=1)
    q_blocks = q_win.reshape(nblocks, WINDOW, heads_win, HEAD)
    scores = (
        jnp.einsum("nqhd,nkd->nhqk", q_blocks, band[..., :HEAD], preferred_element_type=jnp.float32)
        * scale
    )
    q_index = jnp.arange(WINDOW)
    k_index = jnp.arange(3 * WINDOW)
    relative = k_index[None, :] - WINDOW - q_index[:, None]
    first_key = lax.axis_index("sp") * tok - WINDOW
    key_pos = first_key + jnp.arange(nblocks)[:, None] * WINDOW + k_index[None, :]
    inside = (key_pos >= 0) & (key_pos < tok * lax.axis_size("sp"))
    valid = (jnp.abs(relative) <= WINDOW)[None] & inside[:, None, :]
    scores = jnp.where(valid[:, None], scores, -jnp.inf)
    sink_logit = sink[None, :, None, None]
    top_win = jnp.maximum(jnp.max(scores, axis=-1, keepdims=True), sink_logit)
    expo = jnp.exp(scores - top_win)
    weights = expo / (jnp.sum(expo, axis=-1, keepdims=True) + jnp.exp(sink_logit - top_win))
    y_win = jnp.einsum(
        "nhqk,nkd->nqhd",
        weights.astype(jnp.bfloat16),
        band[..., HEAD:],
        preferred_element_type=jnp.float32,
    ).astype(jnp.bfloat16)
    y_win = y_win.reshape(tok, heads_win * HEAD)
    summed = jnp.dot(differential_output, proj_diff, preferred_element_type=jnp.float32)
    return lax.psum_scatter(
        (summed + jnp.dot(y_win, proj_win, preferred_element_type=jnp.float32)).astype(
            jnp.bfloat16
        ),
        "tp",
        scatter_dimension=0,
        tiled=True,
    )


def solution(mesh):
    placed = (
        P(("grp", "sp", "tp"), None),
        P(),
        P("sp", "tp"),
        P("sp", "tp"),
        P("sp", "tp"),
        P("tp"),
        P(),
        P("sp", "tp"),
        P(None, "sp", None),
        P("tp"),
        P("tp", None),
        P("tp", None),
    )
    return jax.shard_map(
        body, mesh=mesh, in_specs=placed, out_specs=P(("grp", "sp", "tp"), None), check_vma=False
    )
```

profile of v0, /device:TPU:0, one launch (start us, length us, event | category | flops | bytes accessed | tf_op | source)
XLA Modules:
  0.0 577.2 jit_solution(6189309447623438986)
XLA Ops:
  6.5 1.7 fusion.16
  8.2 2.5 fusion.18
  15.3 1.9 bitcast_dynamic-update-slice_fusion
  17.3 30.9 %all-gather.5.cloned.1.call-done = bf16[512,4096]{1,0:T(8,128)(2,1)} async-done(((bf16[128,4096]{1,0:T(8,128)(2,1)}), bf16[512,4096]{1,0:T(8,128)(2,1)}) %all-gather.5.cloned.1.call-update) | async-done | bytes 4194320 | tf_op jit(solution)/shard_map/all_gather | solution.py:59
  48.1 324.2 %all-gather.7.cloned.1.call-done = bf16[4096,2304]{1,0:T(8,128)(2,1)} async-done(((bf16[1024,2304]{1,0:T(8,128)(2,1)}), bf16[4096,2304]{1,0:T(8,128)(2,1)}) %all-gather.7.cloned.1.call-update) | async-done | bytes 18874384 | tf_op jit(solution)/shard_map/all_gather | solution.py:57
  372.3 14.4 %convolution_convert_fusion = bf16[512,2304]{1,0:T(8,128)(2,1)S(1)} fusion(bf16[512,4096]{1,0:T(8,128)(2,1)} %all-gather.5.cloned.1.call-done, bf16[4096,2304]{1,0:T(8,128)(2,1)} %all-gather.7.cloned.1.call-done), kind=kOutput, calls=%fused_computation.22 | convolution fusion | flops 9664856064 | bytes 25427968 | tf_op jit(solution)/shard_map/dot_general | solution.py:58
  386.7 1.3 fusion.34
  390.8 1.3 collective-permute-start.1
  396.3 1.6 collective-permute-done.1
  399.5 1.8 fusion.21
  401.3 1.3 copy.30
  402.7 30.4 %all-gather.9.cloned.1.call-done = bf16[2048,512]{1,0:T(8,128)(2,1)} async-done(((bf16[512,512]{1,0:T(8,128)(2,1)}), bf16[2048,512]{1,0:T(8,128)(2,1)}) %all-gather.9.cloned.1.call-update) | async-done | bytes 2097168 | tf_op jit(solution)/shard_map/all_gather | solution.py:77
  433.1 4.0 reshape.116
  437.1 41.4 %all-gather.11.cloned.1.call-done = bf16[2048,512]{1,0:T(8,128)(2,1)} async-done(((bf16[512,512]{1,0:T(8,128)(2,1)}), bf16[2048,512]{1,0:T(8,128)(2,1)}) %all-gather.11.cloned.1.call-update) | async-done | bytes 2097168 | tf_op jit(solution)/shard_map/all_gather | solution.py:78
  478.6 4.0 reshape.118
  482.5 31.8 %while.15 = (s32[]{:T(128)}, f32[2,2,512]{2,1,0:T(2,128)S(1)}, f32[2,2,512]{2,1,0:T(2,128)S(1)}, f32[2,2,512,256]{3,2,1,0:T(8,128)S(1)}, bf16[2,1024,2,2,128]{4,...) while((s32[]{:T(128)}, f32[2,2,512]{2,1,0:T(2,128)S(1)}, ...), condition=%wide.region_4.5_spmd.clone, body=%wide.region_1.4_spmd.clone.sunk | while | flops 1628973056 | bytes 69861520 | solution.py:103
  482.5 1.9 constant_dynamic-slice_fusion.4
  484.5 4.5 bitcast_reduce_fusion.2
  489.0 4.9 fusion.51
  494.0 2.0 constant_dynamic-slice_fusion.5
  495.9 2.5 fusion.53
  498.5 1.9 constant_dynamic-slice_fusion.4
  500.4 4.5 bitcast_reduce_fusion.2
  504.9 4.9 fusion.51
  509.9 2.0 constant_dynamic-slice_fusion.5
  511.9 2.5 fusion.53
  514.4 1.8 copy.26
  516.2 1.9 broadcast_divide_fusion
  518.7 1.6 copy-done.1
  520.3 2.4 fusion.35
  522.7 4.4 add_convert_fusion
  527.1 43.6 %reduce-scatter.2.cloned.1.call-done = bf16[128,4096]{1,0:T(8,128)(2,1)} async-done(((bf16[512,4096]{1,0:T(8,128)(2,1)}), bf16[128,4096]{1,0:T(8,128)(2,1)}) %reduce-scatter.2.cloned.1.call-update) | async-done | bytes 1048592 | tf_op jit(solution)/shard_map/reduce_scatter | solution.py:142
  (73 shorter events, 13.7 us)
Async XLA Ops:
  6.5 4.3 copy-start.4
  6.5 5.4 copy-start.5
  6.5 41.6 %all-gather.5.cloned.1.call-start = ((), (), s32[]{:S(2)}) async-start(), calls=%async_computation.1 | async-start | bytes 5242880 | tf_op jit(solution)/shard_map/all_gather | solution.py:59
  10.7 2.3 copy-start.6
  10.8 361.5 %all-gather.7.cloned.1.call-start = ((), (), s32[]{:S(2)}) async-start(), calls=%async_computation.2 | async-start | bytes 23592960 | tf_op jit(solution)/shard_map/all_gather | solution.py:57
  10.9 3.3 copy-start.7
  17.2 415.9 %all-gather.9.cloned.1.call-start = ((), (), s32[]{:S(2)}) async-start(), calls=%async_computation.3 | async-start | bytes 2621440 | tf_op jit(solution)/shard_map/all_gather | solution.py:77
  386.7 5.5 copy-start.3
  388.0 90.6 %all-gather.11.cloned.1.call-start = ((), (), s32[]{:S(2)}) async-start(), calls=%async_computation.4 | async-start | bytes 2621440 | tf_op jit(solution)/shard_map/all_gather | solution.py:78
  388.6 182.1 %reduce-scatter.2.cloned.1.call-start = ((), (), s32[]{:S(2)}) async-start(), calls=%async_computation.5 | async-start | bytes 5242880 | tf_op jit(solution)/shard_map/reduce_scatter | solution.py:142
  389.5 6.8 %collective-permute-start = (bf16[128,256]{1,0:T(8,128)(2,1)}, bf16[128,256]{1,0:T(8,128)(2,1)S(1)}, u32[]{:S(2)}, u32[]{:S(2)}) collective-permute-start(bf16[128,256]{1,0:T(8,128)(2,1)} %get-tuple-element.101), channel_id=1, source_target_pairs={{0,4},{4,8},{8,12},{1,5},{5,9},{9,13},{2,6},{6,10},{10,14},{3,7},{... | collective-permute-start | bytes 196616 | tf_op jit(solution)/shard_map/ppermute | solution.py:25
  390.8 7.1 %collective-permute-start.1 = (bf16[128,256]{1,0:T(8,128)(2,1)}, bf16[128,256]{1,0:T(8,128)(2,1)S(1)}, u32[]{:S(2)}, u32[]{:S(2)}) collective-permute-start(bf16[128,256]{1,0:T(8,128)(2,1)} %get-tuple-element.102), channel_id=1, source_target_pairs={{4,0},{8,4},{12,8},{5,1},{9,5},{13,9},{6,2},{10,6},{14,10},{7,3},{... | collective-permute-start | bytes 196616 | tf_op jit(solution)/shard_map/ppermute | solution.py:26
  396.2 1.9 copy-start.8
  396.2 1.9 copy-start.9
  398.0 0.7 copy-start.10
  489.0 6.9 %copy-start = (f32[2,2,1024,512]{3,2,1,0:T(8,128)S(1)}, f32[2,2,1024,512]{3,2,1,0:T(8,128)}, u32[]{:S(2)}) copy-start(f32[2,2,1024,512]{3,2,1,0:T(8,128)} %get-tuple-element.159) | copy-start | bytes 25165828 | tf_op jit(solution)/shard_map/while
  504.9 6.9 %copy-start = (f32[2,2,1024,512]{3,2,1,0:T(8,128)S(1)}, f32[2,2,1024,512]{3,2,1,0:T(8,128)}, u32[]{:S(2)}) copy-start(f32[2,2,1024,512]{3,2,1,0:T(8,128)} %get-tuple-element.159) | copy-start | bytes 25165828 | tf_op jit(solution)/shard_map/while
  516.2 1.9 copy-start.11
  516.2 2.2 copy-start.12
  518.1 2.2 copy-start.1
  520.3 2.4 copy-start.2
Sparse Core Ops, SparseCore 0:
  10.9 37.1 all-gather.4
  49.7 322.5 all-gather.6
  388.1 44.9 all-gather.8
  434.5 43.9 all-gather.10
  527.2 43.3 reduce-scatter.1
where the time goes:
time: 578 us; the launch traced here: 577 us
  waiting for transfers between devices  473 us (82%)
  matrix products  37.5 us (6%)
  local copies, waits for them, and re-layouts  32.1 us (6%)
  other arithmetic  18.6 us (3%)
  between operations  13.4 us (2%)
    all_gather x1, waiting for transfers between devices, body(): whole = lax.all_gather(stacked, 'sp', axis=0, tiled=True)  324 us
    reduce_scatter x1, waiting for transfers between devices, body(): lax.psum_scatter((summed + jnp.dot(y_win, proj_win, preferred_element_typ...  43.6 us
    all_gather x1, waiting for transfers between devices, body(): values = lax.all_gather(v_diff, 'sp', axis=0, tiled=True)  41.4 us
    all_gather x1, waiting for transfers between devices, body(): lax.all_gather(normed, 'tp', axis=0, tiled=True)  30.9 us
    all_gather x1, waiting for transfers between devices, body(): keys = lax.all_gather(k_diff, 'sp', axis=0, tiled=True)  30.4 us
    dot_general x1, matrix products, body(): jnp.dot(lax.all_gather(normed, 'tp', axis=0, tiled=True), whole, preferre...  14.4 us
  transfers between devices with their start and end apart: 7, of which 6 were waited for; matrix products, arithmetic and copies ran while one was open for 3% of the time, Pallas kernels for 0%

commit v1 on v0

v1 whole, which is shorter than its diff:
```python
import math

import jax
import jax.numpy as jnp
from jax import lax
from jax.experimental import pallas as pl
from jax.experimental.pallas import tpu as pltpu
from jax.sharding import PartitionSpec as P


HEAD = 128
WIN_HEADS = 16
KV_HEADS = 4
WINDOW = 128
VDIM = 256


EPS = 1e-06


def padded_2(x, sides, width):
    for axis, dim in sides:
        devices, length = (lax.axis_size(axis), x.shape[dim])
        up = [(i, (i + 1) % devices) for i in range(devices - 1)]
        down = [(j, i) for i, j in up]
        last = lax.slice_in_dim(x, length - width, length, axis=dim)
        first = lax.slice_in_dim(x, 0, width, axis=dim)
        before = lax.ppermute(last, axis, up)
        after = lax.ppermute(first, axis, down)
        x = jnp.concatenate([before, x, after], axis=dim)
    return x


def root_mean_square_rows(values, gain):
    return values * lax.rsqrt(jnp.mean(values * values, axis=-1, keepdims=True) + EPS) * gain


def shifted(x, axis, by):
    n = lax.axis_size(axis)
    return lax.ppermute(x, axis, [(i, (i + by) % n) for i in range(n)])


def shift_chip(x, by):
    n = lax.axis_size("tp")
    return lax.ppermute(x, "tp", [(i, (i + 2 * by) % n) for i in range(n)])


def swap_core(x):
    n = lax.axis_size("tp")
    return lax.ppermute(x, "tp", [(i, i ^ 1) for i in range(n)])


def gather_tp(x, axis):
    tp = lax.axis_size("tp")
    chips = tp // 2
    me = lax.axis_index("tp")
    mine = [x] + [shift_chip(x, r) for r in range(1, chips)]
    theirs = [swap_core(piece) for piece in mine]
    out = jnp.zeros(x.shape[:axis] + (tp,) + x.shape[axis:], x.dtype)
    for r in range(chips):
        at = (me - 2 * r) % tp
        out = lax.dynamic_update_slice_in_dim(out, jnp.expand_dims(mine[r], axis), at, axis)
        out = lax.dynamic_update_slice_in_dim(out, jnp.expand_dims(theirs[r], axis), at ^ 1, axis)
    return out


def scatter_tp(x):
    tp = lax.axis_size("tp")
    chips = tp // 2
    me = lax.axis_index("tp")
    core, chip = me % 2, me // 2
    x = x.reshape(chips, 2, x.shape[0] // tp, x.shape[1])
    away = lax.dynamic_index_in_dim(x, 1 - core, 1, keepdims=False).astype(jnp.bfloat16)
    keep = lax.dynamic_index_in_dim(x, core, 1, keepdims=False)
    both = keep + swap_core(away).astype(jnp.float32)
    total = lax.dynamic_index_in_dim(both, chip, 0, keepdims=False)
    for r in range(1, chips):
        sent = lax.dynamic_index_in_dim(both, (chip + r) % chips, 0, keepdims=False)
        total = total + shift_chip(sent.astype(jnp.bfloat16), r).astype(jnp.float32)
    return total.astype(jnp.bfloat16)


def diff_kernel(lam_ref, q_ref, k_ref, v_ref, gain_ref, o_ref):
    factor = HEAD ** (-0.5) * math.log2(math.e)
    maps = []
    for m in range(2):
        cols = slice(m * HEAD, (m + 1) * HEAD)
        scores = lax.dot_general(
            q_ref[:, cols], k_ref[:, cols], (((1,), (1,)), ((), ())),
            preferred_element_type=jnp.float32,
        )
        top = jnp.max(scores, axis=-1, keepdims=True)
        expo = jnp.exp2((scores - top) * factor)
        total = jnp.sum(expo, axis=-1, keepdims=True)
        out = jnp.dot(expo.astype(jnp.bfloat16), v_ref[...], preferred_element_type=jnp.float32)
        maps.append(out / total)
    d = maps[0] - lam_ref[pl.program_id(0)] * maps[1]
    d = d * lax.rsqrt(jnp.mean(d * d, axis=-1, keepdims=True) + EPS) * gain_ref[...]
    o_ref[...] = d.astype(jnp.bfloat16)


def diff_attention(q, kv, lam, gain):
    tok, rows, heads = q.shape[0], kv.shape[0], lam.shape[0]
    tile = math.gcd(tok, max(128, 524288 // rows))
    return pl.pallas_call(
        diff_kernel,
        grid=(heads, tok // tile),
        in_specs=[
            pl.BlockSpec(memory_space=pltpu.SMEM),
            pl.BlockSpec((tile, 2 * HEAD), lambda h, i: (i, h)),
            pl.BlockSpec((rows, 2 * HEAD), lambda h, i: (0, h)),
            pl.BlockSpec((rows, VDIM), lambda h, i: (0, heads + h)),
            pl.BlockSpec((1, VDIM), lambda h, i: (0, 0)),
        ],
        out_specs=pl.BlockSpec((tile, VDIM), lambda h, i: (i, h)),
        out_shape=jax.ShapeDtypeStruct((tok, heads * VDIM), jnp.bfloat16),
        cost_estimate=pl.CostEstimate(
            flops=heads * tok * rows * 2 * 2 * (HEAD + VDIM),
            bytes_accessed=2 * (q.size * 2 + kv.size),
            transcendentals=heads * 2 * tok * rows,
        ),
    )(lam, q, kv, kv, gain.reshape(1, VDIM))


def body(
    tokens,
    norm_gain,
    query_diff,
    key_diff,
    value_diff,
    lam,
    output_norm_gain,
    query_win,
    keyval_win,
    sink,
    proj_diff,
    proj_win,
):
    bf16, f32 = jnp.bfloat16, jnp.float32
    normed = root_mean_square_rows(tokens.astype(f32), norm_gain).astype(bf16)
    heads_win = sink.shape[0]
    group = WIN_HEADS // KV_HEADS
    n = lax.axis_size("sp")
    me = lax.axis_index("sp")
    parts = lax.axis_size("grp")
    part = lax.axis_index("grp")
    local, width = normed.shape
    depth = width // n
    tok = local * lax.axis_size("tp")

    slabs = normed.reshape(local, n, depth)
    across = jnp.zeros((n, local, depth), bf16)
    own = lax.dynamic_index_in_dim(slabs, me, 1, keepdims=True)
    across = lax.dynamic_update_slice_in_dim(across, jnp.swapaxes(own, 0, 1), me, 0)
    for r in range(1, n):
        sent = lax.dynamic_index_in_dim(slabs, (me + r) % n, 1, keepdims=False)
        got = shifted(sent, "sp", r)
        across = lax.dynamic_update_slice_in_dim(across, got[None], (me - r) % n, 0)

    kv_index = lax.axis_index("tp") * heads_win // group
    kv_local = lax.dynamic_index_in_dim(keyval_win, kv_index, 0, keepdims=False)
    stacked = jnp.concatenate([query_diff, query_win, kv_local], axis=1)
    share = stacked.shape[1] // parts
    half = lax.dynamic_slice_in_dim(stacked, part * share, share, axis=1)
    across, half = lax.optimization_barrier((across, half))

    pieces = [shifted(half, "sp", r) for r in range(1, n)]
    all_rows = gather_tp(across, 1).reshape(n * tok, depth)
    rows_all = gather_tp(normed, 0).reshape(tok, width)
    kv_part = jnp.concatenate(
        [
            jnp.dot(all_rows, key_diff, preferred_element_type=f32).astype(bf16),
            jnp.dot(all_rows, value_diff, preferred_element_type=f32).astype(bf16),
        ],
        axis=1,
    )
    kv = lax.psum_scatter(kv_part, "sp", scatter_dimension=0, tiled=True)
    kv = lax.all_gather(kv, "sp", axis=0, tiled=True)

    own_rows = lax.dynamic_slice_in_dim(rows_all, me * depth, depth, axis=1)
    own_sum = jnp.dot(own_rows, stacked, preferred_element_type=f32)
    sums = [jnp.zeros((tok, share), f32) for _ in range(parts)]
    for r in range(1, n):
        piece = pieces[r - 1]
        rows = lax.dynamic_slice_in_dim(rows_all, (me - r) % n * depth, depth, axis=1)
        for j in range(parts):
            block = piece if j == 0 else shifted(piece, "grp", j)
            sums[j] = sums[j] + jnp.dot(rows, block, preferred_element_type=f32)
    ordered = jnp.stack(sums)
    ordered = jnp.concatenate(
        [
            lax.dynamic_index_in_dim(ordered, (part - b) % parts, 0, keepdims=False)
            for b in range(parts)
        ],
        axis=1,
    )
    projected = (own_sum + ordered).astype(bf16)
    first = query_diff.shape[1]
    second = first + query_win.shape[1]
    q_diff, q_win, kv_win = projected[:, :first], projected[:, first:second], projected[:, second:]
    scale = HEAD ** (-0.5)
    padded = padded_2(kv_win, (("sp", 0),), WINDOW)
    nblocks = tok // WINDOW
    blocks = padded.reshape(nblocks + 2, WINDOW, 2 * HEAD)
    band = jnp.concatenate([blocks[:-2], blocks[1:-1], blocks[2:]], axis=1)
    q_blocks = q_win.reshape(nblocks, WINDOW, heads_win, HEAD)
    scores = (
        jnp.einsum("nqhd,nkd->nhqk", q_blocks, band[..., :HEAD], preferred_element_type=jnp.float32)
        * scale
    )
    q_index = jnp.arange(WINDOW)
    k_index = jnp.arange(3 * WINDOW)
    relative = k_index[None, :] - WINDOW - q_index[:, None]
    first_key = lax.axis_index("sp") * tok - WINDOW
    key_pos = first_key + jnp.arange(nblocks)[:, None] * WINDOW + k_index[None, :]
    inside = (key_pos >= 0) & (key_pos < tok * lax.axis_size("sp"))
    valid = (jnp.abs(relative) <= WINDOW)[None] & inside[:, None, :]
    scores = jnp.where(valid[:, None], scores, -jnp.inf)
    sink_logit = sink[None, :, None, None]
    top_win = jnp.maximum(jnp.max(scores, axis=-1, keepdims=True), sink_logit)
    expo = jnp.exp(scores - top_win)
    weights = expo / (jnp.sum(expo, axis=-1, keepdims=True) + jnp.exp(sink_logit - top_win))
    y_win = jnp.einsum(
        "nhqk,nkd->nqhd",
        weights.astype(jnp.bfloat16),
        band[..., HEAD:],
        preferred_element_type=jnp.float32,
    ).astype(jnp.bfloat16)
    y_win = y_win.reshape(tok, heads_win * HEAD)
    summed = jnp.dot(y_win, proj_win, preferred_element_type=jnp.float32)
    differential_output = diff_attention(q_diff, kv, lam, output_norm_gain)
    summed = summed + jnp.dot(differential_output, proj_diff, preferred_element_type=jnp.float32)
    return scatter_tp(summed)


def solution(mesh):
    placed = (
        P(("grp", "sp", "tp"), None),
        P(),
        P("sp", "tp"),
        P("sp", "tp"),
        P("sp", "tp"),
        P("tp"),
        P(),
        P("sp", "tp"),
        P(None, "sp", None),
        P("tp"),
        P("tp", None),
        P("tp", None),
    )
    return jax.shard_map(
        body, mesh=mesh, in_specs=placed, out_specs=P(("grp", "sp", "tp"), None), check_vma=False
    )
```

time: 578 us -> 424 us (0.73)
  waiting for transfers between devices: 473 us -> 229 us
  starting transfers between devices: 2.74 us -> 75.3 us
  Pallas kernels: 0 us -> 11.5 us
    all_gather x4 -> x1, waiting for transfers between devices: 427 us -> 0.01 us  [body(): kv = lax.all_gather(kv, 'sp', axis=0, tiled=True)]
    ppermute x0 -> x17, waiting for transfers between devices: none -> 221 us  [the longest x9 153 us: shifted(): return lax.ppermute(x, axis, [(i, (i + by) % n) for i in range(n)])]
    ppermute x1, starting transfers between devices: 1.28 us -> 50.3 us  [padded_2(): before = lax.ppermute(last, axis, up)]
    reduce_scatter x1, waiting for transfers between devices: 43.6 us -> 2.65 us  [body(): kv = lax.psum_scatter(kv_part, 'sp', scatter_dimension=0, tiled=True)]
    ppermute x0 -> x17, starting transfers between devices: none -> 23.5 us  [the longest x9 18.8 us: shifted(): return lax.ppermute(x, axis, [(i, (i + by) % n) for i in range(n)])]
    pallas_call x0 -> x1, Pallas kernels: none -> 11.5 us  [diff_attention(): pl.pallas_call(diff_kernel, grid=(heads, tok // tile), in_specs=[pl.Block...]
    dynamic_update_slice x0 -> x11, local copies, waits for them, and re-layouts: none -> 10.7 us  [the longest x4 7.46 us: gather_tp(): lax.dynamic_update_slice_in_dim(out, jnp.expand_dims(theirs[r], axis), at...]
    reduce_sum x2 -> x0, other arithmetic: 9.84 us -> none  [one(): total = total * fade + jnp.sum(expo, axis=-1)]
  transfers between devices with their start and end apart: 7 -> 21, of which waited for: 6 -> 13; matrix products, arithmetic and copies ran while one was open for 3% -> 12% of each run, Pallas kernels for 0% -> 0%
where the time goes in v1:
time: 424 us; the launch traced here: 423 us
  waiting for transfers between devices  229 us (54%)
  starting transfers between devices  75.3 us (18%)
  matrix products  40.8 us (10%)
  local copies, waits for them, and re-layouts  34.4 us (8%)
  other arithmetic  17.6 us (4%)
  between operations  13.9 us (3%)
  Pallas kernels  11.5 us (3%)
    ppermute x9, waiting for transfers between devices, shifted(): return lax.ppermute(x, axis, [(i, (i + by) % n) for i in range(n)])  153 us
    ppermute x3, waiting for transfers between devices, shift_chip(): return lax.ppermute(x, 'tp', [(i, (i + 2 * by) % n) for i in range(n)])  63 us
    ppermute x1, starting transfers between devices, padded_2(): before = lax.ppermute(last, axis, up)  50.3 us
    ppermute x9, starting transfers between devices, shifted(): return lax.ppermute(x, axis, [(i, (i + by) % n) for i in range(n)])  18.8 us
    dot_general x6, matrix products, body(): sums[j] = sums[j] + jnp.dot(rows, block, preferred_element_type=f32)  15.8 us
    pallas_call x1, Pallas kernels, diff_attention(): pl.pallas_call(diff_kernel, grid=(heads, tok // tile), in_specs=[pl.Block...  11.5 us
  transfers between devices with their start and end apart: 21, of which 13 were waited for; matrix products, arithmetic and copies ran while one was open for 12% of the time, Pallas kernels for 0%

profile of v1, /device:TPU:0, one launch (start us, length us, event | category | flops | bytes accessed | tf_op | source)
XLA Modules:
  0.0 422.9 jit_solution(14484452591825934497)
XLA Ops:
  16.9 3.1 collective-permute-start.3
  21.8 2.6 collective-permute-start.4
  27.7 3.2 pad_maximum_fusion.1
  31.1 2.5 constant_dynamic-slice_fusion
  34.6 5.4 %collective-permute-done.4 = bf16[128,1024]{1,0:T(8,128)(2,1)} collective-permute-done((bf16[128,1024]{1,0:T(8,128)(2,1)}, bf16[128,1024]{1,0:T(8,128)(2,1)}, u32[]{:S(2)}, u32[]{:S(2)}) %collective-permute-start.4) | collective-permute-done | bytes 262176 | tf_op jit(solution)/shard_map/ppermute | solution.py:40
  42.6 23.4 %collective-permute-done.15 = bf16[4,128,1024]{2,1,0:T(8,128)(2,1)S(1)} collective-permute-done((bf16[4,128,1024]{2,1,0:T(8,128)(2,1)S(1)}, bf16[4,128,1024]{2,1,0:T(8,128)(2,1)S(1)}, u32[]{:S(2)}, u32[]{:S(2)}) %collective-permute-start.15) | collective-permute-done | bytes 1048608 | tf_op jit(solution)/shard_map/ppermute | solution.py:45
  74.9 2.6 pad_maximum_fusion
  80.8 4.2 %collective-permute-start.7 = (bf16[1024,640]{1,0:T(8,128)(2,1)}, bf16[1024,640]{1,0:T(8,128)(2,1)}, u32[]{:S(2)}, u32[]{:S(2)}) collective-permute-start(bf16[1024,640]{1,0:T(8,128)(2,1)} %constant_dynamic-slice_fusion), channel_id=1, source_target_pairs={{0,8},{4,12},{8,0},{12,4},{1,9},{5,13},{9,1},{13,5},{2,10},{6,14},... | collective-permute-start | bytes 3932168 | tf_op jit(solution)/shard_map/ppermute | solution.py:40
  85.1 3.3 collective-permute-start.8
  88.3 15.6 %collective-permute-done.1 = bf16[128,4096]{1,0:T(8,128)(2,1)S(1)} collective-permute-done((bf16[128,4096]{1,0:T(8,128)(2,1)S(1)}, bf16[128,4096]{1,0:T(8,128)(2,1)S(1)}, u32[]{:S(2)}, u32[]{:S(2)}) %collective-permute-start.1) | collective-permute-done | bytes 1048608 | tf_op jit(solution)/shard_map/ppermute | solution.py:45
  107.3 83.5 %collective-permute-done.7 = bf16[1024,640]{1,0:T(8,128)(2,1)} collective-permute-done((bf16[1024,640]{1,0:T(8,128)(2,1)}, bf16[1024,640]{1,0:T(8,128)(2,1)}, u32[]{:S(2)}, u32[]{:S(2)}) %collective-permute-start.7) | collective-permute-done | bytes 1310752 | tf_op jit(solution)/shard_map/ppermute | solution.py:40
  192.4 5.3 %collective-permute-done.8 = bf16[1024,640]{1,0:T(8,128)(2,1)} collective-permute-done((bf16[1024,640]{1,0:T(8,128)(2,1)}, bf16[1024,640]{1,0:T(8,128)(2,1)}, u32[]{:S(2)}, u32[]{:S(2)}) %collective-permute-start.8) | collective-permute-done | bytes 1310752 | tf_op jit(solution)/shard_map/ppermute | solution.py:40
  198.9 42.6 %collective-permute-done.6 = bf16[1024,640]{1,0:T(8,128)(2,1)} collective-permute-done((bf16[1024,640]{1,0:T(8,128)(2,1)}, bf16[1024,640]{1,0:T(8,128)(2,1)}, u32[]{:S(2)}, u32[]{:S(2)}) %collective-permute-start.6) | collective-permute-done | bytes 1310752 | tf_op jit(solution)/shard_map/ppermute | solution.py:40
  243.0 2.7 reduce-scatter.2.cloned.1.call-done
  248.0 2.6 fusion.27
  250.7 2.6 fusion.23
  253.3 2.7 fusion.11
  256.0 2.6 fusion.25
  258.6 2.6 fusion.21
  261.2 16.5 %collective-permute-done.9 = bf16[1024,640]{1,0:T(8,128)(2,1)} collective-permute-done((bf16[1024,640]{1,0:T(8,128)(2,1)}, bf16[1024,640]{1,0:T(8,128)(2,1)}, u32[]{:S(2)}, u32[]{:S(2)}) %collective-permute-start.9) | collective-permute-done | bytes 1310752 | tf_op jit(solution)/shard_map/ppermute | solution.py:40
  277.7 2.7 fusion.12
  281.9 3.7 fusion
  285.7 50.3 %collective-permute-start.12 = (bf16[128,256]{1,0:T(8,128)(2,1)S(1)}, bf16[128,256]{1,0:T(8,128)(2,1)S(1)}, u32[]{:S(2)}, u32[]{:S(2)}) collective-permute-start(bf16[128,256]{1,0:T(8,128)(2,1)S(1)} %get-tuple-element.15), channel_id=1, source_target_pairs={{0,4},{4,8},{8,12},{1,5},{5,9},{9,13},{2,6},{6,10},{10,14},{3,7},{... | collective-permute-start | bytes 196616 | tf_op jit(solution)/shard_map/ppermute | solution.py:28
  339.2 4.8 %collective-permute-done.13 = bf16[128,256]{1,0:T(8,128)(2,1)S(1)} collective-permute-done((bf16[128,256]{1,0:T(8,128)(2,1)S(1)}, bf16[128,256]{1,0:T(8,128)(2,1)S(1)}, u32[]{:S(2)}, u32[]{:S(2)}) %collective-permute-start.13) | collective-permute-done | bytes 65568 | tf_op jit(solution)/shard_map/ppermute | solution.py:29
  346.9 7.8 %fusion.31 = f32[512,4096]{1,0:T(8,128)} fusion(bf16[512,4096]{1,0:T(8,128)(2,1)} %param.23, bf16[64,8,4,128]{3,2,1,0:T(4,128)(2,1)S(1)} %bitcast.116), kind=kOutput, calls=%fused_computation.61 | convolution fusion | flops 2147483648 | bytes 13107200 | tf_op jit(solution)/shard_map/dot_general | solution.py:230
  354.7 11.5 %shard_map.118 = bf16[512,512]{1,0:T(8,128)(2,1)} custom-call(f32[2]{0:T(128)} %lam_ref.1, bf16[512,512]{1,0:T(8,128)(2,1)} %get-tuple-element.13.q_ref, bf16[2048,1024]{1,0:T(8,128)(2,1)} %all-gather.2.cloned.1.call-done.k_ref.v_ref, bf16[2048,1024]{1,0:T(8,128)(2,1)} %all-gather.2.cloned.1.call-done.k_ref.v_ref, f32[1,256]{1,0:T(1,128)} %bitcast.119), custom_call_target="tpu_custom_call" | custom-call | flops 3221225472 | bytes 5242880 | tf_op jit(solution)/shard_map/pallas_call | solution.py:105
  366.2 7.2 %convolution_add_fusion = f32[512,4096]{1,0:T(8,128)S(1)} fusion(f32[512,4096]{1,0:T(8,128)} %fusion.31, bf16[512,512]{1,0:T(8,128)(2,1)} %shard_map.118, bf16[512,4096]{1,0:T(8,128)(2,1)} %param.22), kind=kOutput, calls=%fused_computation | convolution fusion | flops 2149580800 | bytes 21495808 | tf_op jit(solution)/shard_map/dot_general | solution.py:232
  373.4 3.3 copy-done.2
  377.1 4.2 %collective-permute-done.17 = bf16[2,128,4096]{2,1,0:T(8,128)(2,1)} collective-permute-done((bf16[2,128,4096]{2,1,0:T(8,128)(2,1)S(1)}, bf16[2,128,4096]{2,1,0:T(8,128)(2,1)}, u32[]{:S(2)}, u32[]{:S(2)}) %collective-permute-start.17) | collective-permute-done | bytes 2097184 | tf_op jit(solution)/shard_map/ppermute | solution.py:50
  381.3 3.5 bitcast_add_fusion
  389.3 24.0 %collective-permute-done.18 = bf16[128,4096]{1,0:T(8,128)(2,1)S(1)} collective-permute-done((bf16[128,4096]{1,0:T(8,128)(2,1)}, bf16[128,4096]{1,0:T(8,128)(2,1)S(1)}, u32[]{:S(2)}, u32[]{:S(2)}) %collective-permute-start.18) | collective-permute-done | bytes 1048608 | tf_op jit(solution)/shard_map/ppermute | solution.py:45
  413.3 2.8 fusion.7
  (97 shorter events, 53.7 us)
Async XLA Ops:
  6.5 21.1 %copy-start = (bf16[4,1024,256]{2,1,0:T(8,128)(2,1)S(1)}, bf16[4,1024,256]{2,1,0:T(8,128)(2,1)}, u32[]{:S(2)}) copy-start(bf16[4,1024,256]{2,1,0:T(8,128)(2,1)} %param.20) | copy-start | bytes 6291460
  6.5 4.3 %copy-start.4 = (bf16[128,4096]{1,0:T(8,128)(2,1)S(1)}, bf16[128,4096]{1,0:T(8,128)(2,1)}, u32[]{:S(2)}) copy-start(bf16[128,4096]{1,0:T(8,128)(2,1)} %param.12) | copy-start | bytes 3145732
  6.5 4.3 %copy-start.8 = (f32[4096]{0:T(1024)S(1)}, f32[4096]{0:T(1024)}, u32[]{:S(2)}) copy-start(f32[4096]{0:T(1024)} %param.13) | copy-start | bytes 49156
  6.5 239.1 %reduce-scatter.2.cloned.1.call-start = ((), (), s32[]{:S(2)}) async-start(), calls=%async_computation.1 | async-start | bytes 5242880 | tf_op jit(solution)/shard_map/reduce_scatter | solution.py:177
  16.9 16.7 %collective-permute-start.3 = (bf16[128,1024]{1,0:T(8,128)(2,1)}, bf16[128,1024]{1,0:T(8,128)(2,1)}, u32[]{:S(2)}, u32[]{:S(2)}) collective-permute-start(bf16[128,1024]{1,0:T(8,128)(2,1)} %bitcast.8), channel_id=1, source_target_pairs={{0,4},{4,8},{8,12},{12,0},{1,5},{5,9},{9,13},{13,1},{2,6},{6,10},{... | collective-permute-start | bytes 786440 | tf_op jit(solution)/shard_map/ppermute | solution.py:40
  21.8 18.2 %collective-permute-start.4 = (bf16[128,1024]{1,0:T(8,128)(2,1)}, bf16[128,1024]{1,0:T(8,128)(2,1)}, u32[]{:S(2)}, u32[]{:S(2)}) collective-permute-start(bf16[128,1024]{1,0:T(8,128)(2,1)} %bitcast.10), channel_id=1, source_target_pairs={{0,8},{4,12},{8,0},{12,4},{1,9},{5,13},{9,1},{13,5},{2,10},{6,14},... | collective-permute-start | bytes 786440 | tf_op jit(solution)/shard_map/ppermute | solution.py:40
  26.1 14.8 %collective-permute-start.5 = (bf16[128,1024]{1,0:T(8,128)(2,1)}, bf16[128,1024]{1,0:T(8,128)(2,1)S(1)}, u32[]{:S(2)}, u32[]{:S(2)}) collective-permute-start(bf16[128,1024]{1,0:T(8,128)(2,1)} %bitcast.12), channel_id=1, source_target_pairs={{0,12},{4,0},{8,4},{12,8},{1,13},{5,1},{9,5},{13,9},{2,14},{6,2},{... | collective-permute-start | bytes 786440 | tf_op jit(solution)/shard_map/ppermute | solution.py:40
  41.0 25.1 %collective-permute-start.15 = (bf16[4,128,1024]{2,1,0:T(8,128)(2,1)S(1)}, bf16[4,128,1024]{2,1,0:T(8,128)(2,1)S(1)}, u32[]{:S(2)}, u32[]{:S(2)}) collective-permute-start(bf16[4,128,1024]{2,1,0:T(8,128)(2,1)S(1)} %bitcast_dynamic-update-slice_fusion.8), channel_id=1, source_target_pairs={{0,2},{1,3},{2,0},{3,1},{4,6},{5,7},{6,4},{7,5},{8,10},{9,11},{10,... | collective-permute-start | bytes 3145736 | tf_op jit(solution)/shard_map/ppermute | solution.py:45
  42.6 24.1 %collective-permute-start.14 = (bf16[4,128,1024]{2,1,0:T(8,128)(2,1)S(1)}, bf16[4,128,1024]{2,1,0:T(8,128)(2,1)}, u32[]{:S(2)}, u32[]{:S(2)}) collective-permute-start(bf16[4,128,1024]{2,1,0:T(8,128)(2,1)S(1)} %bitcast_dynamic-update-slice_fusion.8), channel_id=1, source_target_pairs={{0,1},{1,0},{2,3},{3,2},{4,5},{5,4},{6,7},{7,6},{8,9},{9,8},{10,11... | collective-permute-start | bytes 3145736 | tf_op jit(solution)/shard_map/ppermute | solution.py:50
  66.0 2.8 collective-permute-start.16
  66.7 3.5 copy-start.10
  70.2 2.4 copy-start.11
  77.5 1.2 copy-start.5
  77.5 277.2 %all-gather.2.cloned.1.call-start = ((), (), s32[]{:S(2)}) async-start(), calls=%async_computation.2 | async-start | bytes 5242880 | tf_op jit(solution)/shard_map/all_gather | solution.py:178
  78.7 25.2 %collective-permute-start.1 = (bf16[128,4096]{1,0:T(8,128)(2,1)S(1)}, bf16[128,4096]{1,0:T(8,128)(2,1)S(1)}, u32[]{:S(2)}, u32[]{:S(2)}) collective-permute-start(bf16[128,4096]{1,0:T(8,128)(2,1)S(1)} %copy-done.5), channel_id=1, source_target_pairs={{0,2},{1,3},{2,0},{3,1},{4,6},{5,7},{6,4},{7,5},{8,10},{9,11},{10,... | collective-permute-start | bytes 3145736 | tf_op jit(solution)/shard_map/ppermute | solution.py:45
  80.3 23.7 %collective-permute-start = (bf16[128,4096]{1,0:T(8,128)(2,1)S(1)}, bf16[128,4096]{1,0:T(8,128)(2,1)}, u32[]{:S(2)}, u32[]{:S(2)}) collective-permute-start(bf16[128,4096]{1,0:T(8,128)(2,1)S(1)} %copy-done.5), channel_id=1, source_target_pairs={{0,1},{1,0},{2,3},{3,2},{4,5},{5,4},{6,7},{7,6},{8,9},{9,8},{10,11... | collective-permute-start | bytes 3145736 | tf_op jit(solution)/shard_map/ppermute | solution.py:50
  80.8 110.0 %collective-permute-start.7 = (bf16[1024,640]{1,0:T(8,128)(2,1)}, bf16[1024,640]{1,0:T(8,128)(2,1)}, u32[]{:S(2)}, u32[]{:S(2)}) collective-permute-start(bf16[1024,640]{1,0:T(8,128)(2,1)} %constant_dynamic-slice_fusion), channel_id=1, source_target_pairs={{0,8},{4,12},{8,0},{12,4},{1,9},{5,13},{9,1},{13,5},{2,10},{6,14},... | collective-permute-start | bytes 3932168 | tf_op jit(solution)/shard_map/ppermute | solution.py:40
  85.1 112.6 %collective-permute-start.8 = (bf16[1024,640]{1,0:T(8,128)(2,1)}, bf16[1024,640]{1,0:T(8,128)(2,1)}, u32[]{:S(2)}, u32[]{:S(2)}) collective-permute-start(bf16[1024,640]{1,0:T(8,128)(2,1)} %constant_dynamic-slice_fusion), channel_id=1, source_target_pairs={{0,12},{4,0},{8,4},{12,8},{1,13},{5,1},{9,5},{13,9},{2,14},{6,2},{... | collective-permute-start | bytes 3932168 | tf_op jit(solution)/shard_map/ppermute | solution.py:40
  88.3 153.1 %collective-permute-start.6 = (bf16[1024,640]{1,0:T(8,128)(2,1)}, bf16[1024,640]{1,0:T(8,128)(2,1)}, u32[]{:S(2)}, u32[]{:S(2)}) collective-permute-start(bf16[1024,640]{1,0:T(8,128)(2,1)} %constant_dynamic-slice_fusion), channel_id=1, source_target_pairs={{0,4},{4,8},{8,12},{12,0},{1,5},{5,9},{9,13},{13,1},{2,6},{6,10},{... | collective-permute-start | bytes 3932168 | tf_op jit(solution)/shard_map/ppermute | solution.py:40
  104.0 141.7 %collective-permute-start.2 = (bf16[128,4096]{1,0:T(8,128)(2,1)S(1)}, bf16[128,4096]{1,0:T(8,128)(2,1)}, u32[]{:S(2)}, u32[]{:S(2)}) collective-permute-start(bf16[128,4096]{1,0:T(8,128)(2,1)S(1)} %collective-permute-done.1), channel_id=1, source_target_pairs={{0,1},{1,0},{2,3},{3,2},{4,5},{5,4},{6,7},{7,6},{8,9},{9,8},{10,11... | collective-permute-start | bytes 3145736 | tf_op jit(solution)/shard_map/ppermute | solution.py:50
  190.8 65.1 %collective-permute-start.10 = (bf16[1024,640]{1,0:T(8,128)(2,1)}, bf16[1024,640]{1,0:T(8,128)(2,1)}, u32[]{:S(2)}, u32[]{:S(2)}) collective-permute-start(bf16[1024,640]{1,0:T(8,128)(2,1)} %collective-permute-done.7), channel_id=1, source_target_pairs={{0,16},{16,0},{1,17},{17,1},{2,18},{18,2},{3,19},{19,3},{4,20},{20... | collective-permute-start | bytes 3932168 | tf_op jit(solution)/shard_map/ppermute | solution.py:40
  197.6 61.0 %collective-permute-start.11 = (bf16[1024,640]{1,0:T(8,128)(2,1)}, bf16[1024,640]{1,0:T(8,128)(2,1)}, u32[]{:S(2)}, u32[]{:S(2)}) collective-permute-start(bf16[1024,640]{1,0:T(8,128)(2,1)} %collective-permute-done.8), channel_id=1, source_target_pairs={{0,16},{16,0},{1,17},{17,1},{2,18},{18,2},{3,19},{19,3},{4,20},{20... | collective-permute-start | bytes 3932168 | tf_op jit(solution)/shard_map/ppermute | solution.py:40
  241.5 36.2 %collective-permute-start.9 = (bf16[1024,640]{1,0:T(8,128)(2,1)}, bf16[1024,640]{1,0:T(8,128)(2,1)}, u32[]{:S(2)}, u32[]{:S(2)}) collective-permute-start(bf16[1024,640]{1,0:T(8,128)(2,1)} %collective-permute-done.6), channel_id=1, source_target_pairs={{0,16},{16,0},{1,17},{17,1},{2,18},{18,2},{3,19},{19,3},{4,20},{20... | collective-permute-start | bytes 3932168 | tf_op jit(solution)/shard_map/ppermute | solution.py:40
  280.4 1.2 copy-start.6
  280.4 1.5 copy-start.7
  285.7 53.5 %collective-permute-start.12 = (bf16[128,256]{1,0:T(8,128)(2,1)S(1)}, bf16[128,256]{1,0:T(8,128)(2,1)S(1)}, u32[]{:S(2)}, u32[]{:S(2)}) collective-permute-start(bf16[128,256]{1,0:T(8,128)(2,1)S(1)} %get-tuple-element.15), channel_id=1, source_target_pairs={{0,4},{4,8},{8,12},{1,5},{5,9},{9,13},{2,6},{6,10},{10,14},{3,7},{... | collective-permute-start | bytes 196616 | tf_op jit(solution)/shard_map/ppermute | solution.py:28
  335.9 8.1 %collective-permute-start.13 = (bf16[128,256]{1,0:T(8,128)(2,1)S(1)}, bf16[128,256]{1,0:T(8,128)(2,1)S(1)}, u32[]{:S(2)}, u32[]{:S(2)}) collective-permute-start(bf16[128,256]{1,0:T(8,128)(2,1)S(1)} %get-tuple-element.16), channel_id=1, source_target_pairs={{4,0},{8,4},{12,8},{5,1},{9,5},{13,9},{6,2},{10,6},{14,10},{7,3},{... | collective-permute-start | bytes 196616 | tf_op jit(solution)/shard_map/ppermute | solution.py:29
  373.4 3.3 copy-start.2
  377.0 4.4 %collective-permute-start.17 = (bf16[2,128,4096]{2,1,0:T(8,128)(2,1)S(1)}, bf16[2,128,4096]{2,1,0:T(8,128)(2,1)}, u32[]{:S(2)}, u32[]{:S(2)}) collective-permute-start(bf16[2,128,4096]{2,1,0:T(8,128)(2,1)S(1)} %fusion.6), channel_id=1, source_target_pairs={{0,1},{1,0},{2,3},{3,2},{4,5},{5,4},{6,7},{7,6},{8,9},{9,8},{10,11... | collective-permute-start | bytes 6291464 | tf_op jit(solution)/shard_map/ppermute | solution.py:50
  381.3 34.7 %copy-start.1 = (bf16[4,1024,256]{2,1,0:T(8,128)(2,1)S(1)}, bf16[4,1024,256]{2,1,0:T(8,128)(2,1)}, u32[]{:S(2)}) copy-start(bf16[4,1024,256]{2,1,0:T(8,128)(2,1)} %param.20) | copy-start | bytes 6291460
  384.8 2.0 copy-start.3
  387.9 25.4 %collective-permute-start.18 = (bf16[128,4096]{1,0:T(8,128)(2,1)}, bf16[128,4096]{1,0:T(8,128)(2,1)S(1)}, u32[]{:S(2)}, u32[]{:S(2)}) collective-permute-start(bf16[128,4096]{1,0:T(8,128)(2,1)} %fusion.19), channel_id=1, source_target_pairs={{0,2},{1,3},{2,0},{3,1},{4,6},{5,7},{6,4},{7,5},{8,10},{9,11},{10,... | collective-permute-start | bytes 3145736 | tf_op jit(solution)/shard_map/ppermute | solution.py:45
  (1 other events, 0.7 us)
Sparse Core Ops, SparseCore 0:
  77.7 167.8 reduce-scatter.1
  247.2 101.4 all-gather.1
